TPU v7x, 32 devices: a whole 2x2x4 slice. The times are simulated.
32 devices in a mesh: grp: 2 (over y), fs: 4 (over z), tp: 4 (over x, core).
Axes of the slice: x: 2, y: 2, z: 4, core: 2. Of those that a mesh axis runs over, the one named last changes fastest.
Arguments:
- layer_input: bfloat16 [3072, 2048], P(('grp', 'fs'), 'tp'), parts along dimension 0, may hold values from -6 to 6
- first_gain: bfloat16 [1, 2048], P(None, 'tp'), may hold values from 0.099609375 to 1.8984375
- ffn_gate_w: bfloat16 [2048, 6144], P('fs', 'tp'), may hold values from -0.125 to 0.125
- ffn_up_w: bfloat16 [2048, 6144], P('fs', 'tp'), may hold values from -0.125 to 0.125
- ffn_down_w: bfloat16 [6144, 2048], P('tp', 'fs'), may hold values from -0.078125 to 0.078125
- mixer_gain: bfloat16 [1, 2048], P(None, 'tp'), may hold values from 0.099609375 to 1.8984375
- pool_in_w: bfloat16 [2048, 1024], P('fs', 'tp'), may hold values from -0.125 to 0.125
- mixer_gate_w: bfloat16 [2048, 2048], P('fs', 'tp'), may hold values from -0.125 to 0.125
- group_mix_w: bfloat16 [8, 128, 128], P('tp'), may hold values from -0.5 to 0.5
- pool_scale: float32 [1, 1024], P(None, 'tp'), may hold values from 0.1 to 1.9
- mixer_out_w: bfloat16 [1024, 2048], P('tp', 'fs'), may hold values from -0.1875 to 0.1875
- second_gain: bfloat16 [1, 2048], P(None, 'tp'), may hold values from 0.099609375 to 1.8984375
Outputs:
- layer_output: bfloat16 [3072, 2048], P(('grp', 'fs'), 'tp'), parts along dimension 0
There are 2 independent parts, one for each index of `grp`. A program takes and returns all parts, laid end to end along the dimension named above; an argument that names none is the same for every part. Nothing has to cross between parts.
All inputs are finite; a program needn't handle non-finite values.
Results may differ from a plain program's by a relative error of at most 0.015.
Values may be sent and summed in bfloat16 or wider, within the bound.
No kernel may reach another device: no remote copies, remote signals or barrier semaphores. Data moves between devices by JAX's collectives and lax.ppermute only.
A program may use at most 64 MiB of HBM per device.

v0:
```python
import jax
import jax.numpy as jnp
from jax import lax
from jax.sharding import PartitionSpec as P


def shift(size, step):
    return [(i, (i + step) % size) for i in range(size)]


def swap(size):
    return [(i, i ^ 1) for i in range(size)]


def per_device(
    layer_input,
    first_gain,
    ffn_gate_w,
    ffn_up_w,
    ffn_down_w,
    mixer_gain,
    pool_in_w,
    mixer_gate_w,
    group_mix_w,
    pool_scale,
    mixer_out_w,
    second_gain,
):
    n_grp, n_fs, n_tp = (lax.axis_size(name) for name in ("grp", "fs", "tp"))
    n_chip = n_tp // 2
    y, z, t = (lax.axis_index(name) for name in ("grp", "fs", "tp"))
    chip, core = (t // 2, t % 2)
    rows, shard = layer_input.shape
    width = shard * n_tp
    block = width // n_fs

    def pieces_of(weight, axis):
        part = weight.shape[axis] // n_grp
        own = [
            lax.dynamic_slice_in_dim(weight, (y - k) % n_grp * part, part, axis)
            for k in range(n_grp)
        ]
        gathered, current = ([own], own[0])
        for _ in range(n_fs - 1):
            current = lax.ppermute(current, "fs", shift(n_fs, 1))
            gathered.append(
                [current] + [lax.ppermute(current, "grp", shift(n_grp, k)) for k in range(1, n_grp)]
            )
        return gathered

    def absolute(weight, axis, split):
        gathered = pieces_of(weight, split)
        shape = list(weight.shape)
        shape[axis] *= n_fs
        whole = jnp.zeros(shape, weight.dtype)
        for s, parts in enumerate(gathered):
            for k, part in enumerate(parts):
                start = [0, 0]
                start[axis] = (z - s) % n_fs * weight.shape[axis]
                start[split] = start[split] + (y - k) % n_grp * part.shape[split]
                whole = lax.dynamic_update_slice(whole, part, start)
        return whole

    def gather_tp(value):
        pieces = [(t, value), (t ^ 1, lax.ppermute(value, "tp", swap(n_tp)))]
        for k in range(1, n_chip):
            far = lax.ppermute(value, "tp", shift(n_tp, 2 * k))
            source = (t - 2 * k) % n_tp
            pieces.append((source, far))
            pieces.append((source ^ 1, lax.ppermute(far, "tp", swap(n_tp))))
        whole = jnp.zeros((value.shape[0], value.shape[1] * n_tp), value.dtype)
        for source, piece in pieces:
            whole = lax.dynamic_update_slice(whole, piece, (0, source * value.shape[1]))
        return whole

    def scatter_tp(partial):

        def at(index):
            return lax.dynamic_slice_in_dim(partial, index * shard, shard, 1)

        total = None
        for k in list(range(1, n_chip)) + [0]:
            there = (chip + k) % n_chip * 2
            other = lax.ppermute(at(there + (1 - core)), "tp", swap(n_tp))
            pair = at(there + core).astype(jnp.float32) + other.astype(jnp.float32)
            if k:
                pair = lax.ppermute(pair.astype(jnp.bfloat16), "tp", shift(n_tp, 2 * k)).astype(
                    jnp.float32
                )
            total = pair if total is None else total + pair
        return total

    def norm_rows(values, gain):
        whole = gather_tp(values)
        gain_whole = lax.all_gather(gain, "tp", axis=1, tiled=True)
        widened = whole.astype(jnp.float32)
        scaled = (widened * gain_whole.astype(jnp.float32)).astype(jnp.bfloat16)
        factor = lax.rsqrt(jnp.mean(widened * widened, axis=1, keepdims=True) + 1e-06)
        return (scaled, factor)

    gate_pieces = pieces_of(ffn_gate_w, 1)
    up_pieces = pieces_of(ffn_up_w, 1)
    down_pieces = pieces_of(ffn_down_w, 0)

    def feed_forward(values, gain):
        scaled, factor = norm_rows(values, gain)
        inputs = [
            lax.dynamic_slice_in_dim(scaled, (z - s) % n_fs * block, block, 1) for s in range(n_fs)
        ]

        def project(gathered, k):
            total = None
            for s in range(n_fs):
                product = jnp.dot(inputs[s], gathered[s][k], preferred_element_type=jnp.float32)
                total = product if total is None else total + product
            return total

        hidden = [
            (
                jax.nn.silu(factor * project(gate_pieces, k)) * (factor * project(up_pieces, k))
            ).astype(jnp.bfloat16)
            for k in range(n_grp)
        ]
        out = jnp.zeros((rows, width), jnp.bfloat16)
        for s in range(n_fs):
            product = None
            for k in range(n_grp):
                term = jnp.dot(hidden[k], down_pieces[s][k], preferred_element_type=jnp.float32)
                product = term if product is None else product + term
            out = lax.dynamic_update_slice(
                out, product.astype(jnp.bfloat16), (0, (z - s) % n_fs * block)
            )
        return scatter_tp(out)

    first = (layer_input.astype(jnp.float32) + 0.5 * feed_forward(layer_input, first_gain)).astype(
        jnp.bfloat16
    )
    pool_in = absolute(pool_in_w, 0, 0)
    mixer_gate = absolute(mixer_gate_w, 0, 0)
    mixer_out = absolute(mixer_out_w, 1, 0)
    scaled, factor = norm_rows(first, mixer_gain)
    pool_pre = (factor * jnp.dot(scaled, pool_in, preferred_element_type=jnp.float32)).astype(
        jnp.bfloat16
    )
    gate_logit = factor * jnp.dot(scaled, mixer_gate, preferred_element_type=jnp.float32)
    groups, group_width = group_mix_w.shape[:2]
    position = lax.broadcasted_iota(jnp.int32, (rows, rows), 0)
    back = position - lax.broadcasted_iota(jnp.int32, (rows, rows), 1)
    row = lax.broadcasted_iota(jnp.int32, (rows, 1), 0)
    pooled = []
    for g in range(groups):
        window = 2 ** (1 + (t * groups + g) % 4)
        band = ((back >= 0) & (back < window)).astype(jnp.bfloat16)
        values = pool_pre[:, g * group_width : (g + 1) * group_width]
        sums = jnp.dot(band, values, preferred_element_type=jnp.float32)
        count = jnp.minimum(row + 1, window).astype(jnp.float32)
        trail = (sums / count - values.astype(jnp.float32)).astype(jnp.bfloat16)
        mixed = jnp.dot(trail, group_mix_w[g], preferred_element_type=jnp.float32)
        pooled.append(mixed)
    pooled = (jnp.concatenate(pooled, axis=1) * pool_scale).astype(jnp.bfloat16)
    lifted = scatter_tp(
        jnp.dot(pooled, mixer_out, preferred_element_type=jnp.float32).astype(jnp.bfloat16)
    )
    second = (first.astype(jnp.float32) + jax.nn.sigmoid(gate_logit) * lifted).astype(jnp.bfloat16)
    result = second.astype(jnp.float32) + 0.5 * feed_forward(second, second_gain)
    return result.astype(jnp.bfloat16)


def solution(mesh):
    return jax.shard_map(
        per_device,
        mesh=mesh,
        in_specs=(
            P(("grp", "fs"), "tp"),
            P(None, "tp"),
            P("fs", "tp"),
            P("fs", "tp"),
            P("tp", "fs"),
            P(None, "tp"),
            P("fs", "tp"),
            P("fs", "tp"),
            P("tp", None, None),
            P(None, "tp"),
            P("tp", "fs"),
            P(None, "tp"),
        ),
        out_specs=P(("grp", "fs"), "tp"),
        check_vma=False,
    )
```

profile of v0, /device:TPU:0, one launch (start us, length us, event | category | flops | bytes accessed | tf_op | source)
XLA Modules:
  0.0 356.5 jit_solution(13257093705416114040)
XLA Ops:
  0.0 3.0 collective-permute-start.1
  7.6 4.8 %collective-permute-done.1 = bf16[384,512]{1,0:T(8,128)(2,1)} collective-permute-done((bf16[384,512]{1,0:T(8,128)(2,1)}, bf16[384,512]{1,0:T(8,128)(2,1)}, u32[]{:S(2)}, u32[]{:S(2)}) %collective-permute-start.1) | collective-permute-done | bytes 393248 | tf_op jit(solution)/shard_map/ppermute | solution.py:67
  15.2 5.2 %all_gather.9 = bf16[1,2048]{1,0:T(2,128)(2,1)S(1)} all-gather(bf16[1,512]{1,0:T(2,128)(2,1)S(1)} %copy-done.40), channel_id=1, replica_groups=mesh['grp'=2,'fs'=4,'tp'=4] {'tp'}, dimensions={1}, use_global_device_ids=true | all-gather | bytes 5120 | tf_op jit(solution)/shard_map/all_gather | solution.py:95
  22.9 3.8 %collective-permute-done.3 = bf16[512,768]{1,0:T(8,128)(2,1)} collective-permute-done((bf16[512,768]{1,0:T(8,128)(2,1)S(1)}, bf16[512,768]{1,0:T(8,128)(2,1)}, u32[]{:S(2)}, u32[]{:S(2)}) %collective-permute-start.3) | collective-permute-done | bytes 786464 | tf_op jit(solution)/shard_map/ppermute | solution.py:45
  30.8 12.8 %collective-permute-done.6 = bf16[512,768]{1,0:T(8,128)(2,1)} collective-permute-done((bf16[512,768]{1,0:T(8,128)(2,1)S(1)}, bf16[512,768]{1,0:T(8,128)(2,1)}, u32[]{:S(2)}, u32[]{:S(2)}) %collective-permute-start.6) | collective-permute-done | bytes 786464 | tf_op jit(solution)/shard_map/ppermute | solution.py:45
  49.4 10.9 %collective-permute-done.15 = bf16[768,512]{1,0:T(8,128)(2,1)} collective-permute-done((bf16[768,512]{1,0:T(8,128)(2,1)}, bf16[768,512]{1,0:T(8,128)(2,1)}, u32[]{:S(2)}, u32[]{:S(2)}) %collective-permute-start.15) | collective-permute-done | bytes 786464 | tf_op jit(solution)/shard_map/ppermute | solution.py:45
  62.0 15.1 %collective-permute-done.4 = bf16[512,768]{1,0:T(8,128)(2,1)S(1)} collective-permute-done((bf16[512,768]{1,0:T(8,128)(2,1)}, bf16[512,768]{1,0:T(8,128)(2,1)S(1)}, u32[]{:S(2)}, u32[]{:S(2)}) %collective-permute-start.4) | collective-permute-done | bytes 786464 | tf_op jit(solution)/shard_map/ppermute | solution.py:45
  79.6 14.4 %collective-permute-done.7 = bf16[512,768]{1,0:T(8,128)(2,1)S(1)} collective-permute-done((bf16[512,768]{1,0:T(8,128)(2,1)}, bf16[512,768]{1,0:T(8,128)(2,1)S(1)}, u32[]{:S(2)}, u32[]{:S(2)}) %collective-permute-start.7) | collective-permute-done | bytes 786464 | tf_op jit(solution)/shard_map/ppermute | solution.py:45
  96.3 14.5 %collective-permute-done.17 = bf16[768,512]{1,0:T(8,128)(2,1)S(1)} collective-permute-done((bf16[768,512]{1,0:T(8,128)(2,1)}, bf16[768,512]{1,0:T(8,128)(2,1)S(1)}, u32[]{:S(2)}, u32[]{:S(2)}) %collective-permute-start.17) | collective-permute-done | bytes 786464 | tf_op jit(solution)/shard_map/ppermute | solution.py:45
  113.5 14.2 %collective-permute-done.5 = bf16[512,768]{1,0:T(8,128)(2,1)S(1)} collective-permute-done((bf16[512,768]{1,0:T(8,128)(2,1)S(1)}, bf16[512,768]{1,0:T(8,128)(2,1)S(1)}, u32[]{:S(2)}, u32[]{:S(2)}) %collective-permute-start.5) | collective-permute-done | bytes 786464 | tf_op jit(solution)/shard_map/ppermute | solution.py:45
  128.2 16.3 %collective-permute-done.8 = bf16[512,768]{1,0:T(8,128)(2,1)S(1)} collective-permute-done((bf16[512,768]{1,0:T(8,128)(2,1)S(1)}, bf16[512,768]{1,0:T(8,128)(2,1)S(1)}, u32[]{:S(2)}, u32[]{:S(2)}) %collective-permute-start.8) | collective-permute-done | bytes 786464 | tf_op jit(solution)/shard_map/ppermute | solution.py:45
  150.4 9.6 %collective-permute-done.19 = bf16[768,512]{1,0:T(8,128)(2,1)S(1)} collective-permute-done((bf16[768,512]{1,0:T(8,128)(2,1)S(1)}, bf16[768,512]{1,0:T(8,128)(2,1)S(1)}, u32[]{:S(2)}, u32[]{:S(2)}) %collective-permute-start.19) | collective-permute-done | bytes 786464 | tf_op jit(solution)/shard_map/ppermute | solution.py:45
  164.0 16.4 %collective-permute-done.14 = bf16[512,768]{1,0:T(8,128)(2,1)S(1)} collective-permute-done((bf16[512,768]{1,0:T(8,128)(2,1)S(1)}, bf16[512,768]{1,0:T(8,128)(2,1)S(1)}, u32[]{:S(2)}, u32[]{:S(2)}) %collective-permute-start.14) | collective-permute-done | bytes 786464 | tf_op jit(solution)/shard_map/ppermute | solution.py:47
  183.0 12.1 %collective-permute-done.20 = bf16[768,512]{1,0:T(8,128)(2,1)S(1)} collective-permute-done((bf16[768,512]{1,0:T(8,128)(2,1)S(1)}, bf16[768,512]{1,0:T(8,128)(2,1)S(1)}, u32[]{:S(2)}, u32[]{:S(2)}) %collective-permute-start.20) | collective-permute-done | bytes 786464 | tf_op jit(solution)/shard_map/ppermute | solution.py:47
  212.4 10.5 %all_gather.10 = bf16[1,2048]{1,0:T(2,128)(2,1)S(1)} all-gather(bf16[1,512]{1,0:T(2,128)(2,1)S(1)} %copy-done.41), channel_id=1, replica_groups=mesh['grp'=2,'fs'=4,'tp'=4] {'tp'}, dimensions={1}, use_global_device_ids=true | all-gather | bytes 5120 | tf_op jit(solution)/shard_map/all_gather | solution.py:95
  243.0 3.4 dynamic_update_slice.164
  256.6 3.4 dynamic_update_slice.166
  271.3 3.4 collective-permute-start.28
  277.1 4.9 %collective-permute-done.28 = bf16[256,512]{1,0:T(8,128)(2,1)S(1)} collective-permute-done((bf16[256,512]{1,0:T(8,128)(2,1)}, bf16[256,512]{1,0:T(8,128)(2,1)S(1)}, u32[]{:S(2)}, u32[]{:S(2)}) %collective-permute-start.28) | collective-permute-done | bytes 262176 | tf_op jit(solution)/shard_map/ppermute | solution.py:47
  289.9 3.1 collective-permute-done.32
  293.7 3.3 collective-permute-done.46
  301.4 9.4 %collective-permute-done.49 = bf16[384,512]{1,0:T(8,128)(2,1)S(1)} collective-permute-done((bf16[384,512]{1,0:T(8,128)(2,1)S(1)}, bf16[384,512]{1,0:T(8,128)(2,1)S(1)}, u32[]{:S(2)}, u32[]{:S(2)}) %collective-permute-start.49) | collective-permute-done | bytes 393248 | tf_op jit(solution)/shard_map/ppermute | solution.py:67
  310.8 5.4 %all_gather.11 = bf16[1,2048]{1,0:T(2,128)(2,1)S(1)} all-gather(bf16[1,512]{1,0:T(2,128)(2,1)S(1)} %copy-done.42), channel_id=1, replica_groups=mesh['grp'=2,'fs'=4,'tp'=4] {'tp'}, dimensions={1}, use_global_device_ids=true | all-gather | bytes 5120 | tf_op jit(solution)/shard_map/all_gather | solution.py:95
  345.4 10.1 %collective-permute-done.52 = bf16[384,512]{1,0:T(8,128)(2,1)S(1)} collective-permute-done((bf16[384,512]{1,0:T(8,128)(2,1)S(1)}, bf16[384,512]{1,0:T(8,128)(2,1)S(1)}, u32[]{:S(2)}, u32[]{:S(2)}) %collective-permute-start.52) | collective-permute-done | bytes 393248 | tf_op jit(solution)/shard_map/ppermute | solution.py:87
  (304 shorter events, 145.2 us)
Async XLA Ops:
  4.3 22.4 %collective-permute-start.3 = (bf16[512,768]{1,0:T(8,128)(2,1)S(1)}, bf16[512,768]{1,0:T(8,128)(2,1)}, u32[]{:S(2)}, u32[]{:S(2)}) collective-permute-start(bf16[512,768]{1,0:T(8,128)(2,1)S(1)} %constant_dynamic-slice_fusion.11), channel_id=1, source_target_pairs={{0,4},{4,8},{8,12},{12,0},{1,5},{5,9},{9,13},{13,1},{2,6},{6,10},{... | collective-permute-start | bytes 2359304 | tf_op jit(solution)/shard_map/ppermute | solution.py:45
  6.0 37.5 %collective-permute-start.6 = (bf16[512,768]{1,0:T(8,128)(2,1)S(1)}, bf16[512,768]{1,0:T(8,128)(2,1)}, u32[]{:S(2)}, u32[]{:S(2)}) collective-permute-start(bf16[512,768]{1,0:T(8,128)(2,1)S(1)} %constant_dynamic-slice_fusion.10), channel_id=1, source_target_pairs={{0,4},{4,8},{8,12},{12,0},{1,5},{5,9},{9,13},{13,1},{2,6},{6,10},{... | collective-permute-start | bytes 2359304 | tf_op jit(solution)/shard_map/ppermute | solution.py:45
  13.4 47.0 %collective-permute-start.15 = (bf16[768,512]{1,0:T(8,128)(2,1)}, bf16[768,512]{1,0:T(8,128)(2,1)}, u32[]{:S(2)}, u32[]{:S(2)}) collective-permute-start(bf16[768,512]{1,0:T(8,128)(2,1)} %constant_dynamic-slice_fusion.9), channel_id=1, source_target_pairs={{0,4},{4,8},{8,12},{12,0},{1,5},{5,9},{9,13},{13,1},{2,6},{6,10},{... | collective-permute-start | bytes 2359304 | tf_op jit(solution)/shard_map/ppermute | solution.py:45
  26.7 35.2 %collective-permute-start.9 = (bf16[512,768]{1,0:T(8,128)(2,1)}, bf16[512,768]{1,0:T(8,128)(2,1)S(1)}, u32[]{:S(2)}, u32[]{:S(2)}) collective-permute-start(bf16[512,768]{1,0:T(8,128)(2,1)} %collective-permute-done.3), channel_id=1, source_target_pairs={{0,16},{16,0},{1,17},{17,1},{2,18},{18,2},{3,19},{19,3},{4,20},{20... | collective-permute-start | bytes 2359304 | tf_op jit(solution)/shard_map/ppermute | solution.py:47
  28.2 48.9 %collective-permute-start.4 = (bf16[512,768]{1,0:T(8,128)(2,1)}, bf16[512,768]{1,0:T(8,128)(2,1)S(1)}, u32[]{:S(2)}, u32[]{:S(2)}) collective-permute-start(bf16[512,768]{1,0:T(8,128)(2,1)} %collective-permute-done.3), channel_id=1, source_target_pairs={{0,4},{4,8},{8,12},{12,0},{1,5},{5,9},{9,13},{13,1},{2,6},{6,10},{... | collective-permute-start | bytes 2359304 | tf_op jit(solution)/shard_map/ppermute | solution.py:45
  43.5 50.5 %collective-permute-start.7 = (bf16[512,768]{1,0:T(8,128)(2,1)}, bf16[512,768]{1,0:T(8,128)(2,1)S(1)}, u32[]{:S(2)}, u32[]{:S(2)}) collective-permute-start(bf16[512,768]{1,0:T(8,128)(2,1)} %collective-permute-done.6), channel_id=1, source_target_pairs={{0,4},{4,8},{8,12},{12,0},{1,5},{5,9},{9,13},{13,1},{2,6},{6,10},{... | collective-permute-start | bytes 2359304 | tf_op jit(solution)/shard_map/ppermute | solution.py:45
  47.9 46.6 %collective-permute-start.12 = (bf16[512,768]{1,0:T(8,128)(2,1)}, bf16[512,768]{1,0:T(8,128)(2,1)S(1)}, u32[]{:S(2)}, u32[]{:S(2)}) collective-permute-start(bf16[512,768]{1,0:T(8,128)(2,1)} %collective-permute-done.6), channel_id=1, source_target_pairs={{0,16},{16,0},{1,17},{17,1},{2,18},{18,2},{3,19},{19,3},{4,20},{20... | collective-permute-start | bytes 2359304 | tf_op jit(solution)/shard_map/ppermute | solution.py:47
  60.4 121.7 %collective-permute-start.16 = (bf16[768,512]{1,0:T(8,128)(2,1)}, bf16[768,512]{1,0:T(8,128)(2,1)S(1)}, u32[]{:S(2)}, u32[]{:S(2)}) collective-permute-start(bf16[768,512]{1,0:T(8,128)(2,1)} %collective-permute-done.15), channel_id=1, source_target_pairs={{0,16},{16,0},{1,17},{17,1},{2,18},{18,2},{3,19},{19,3},{4,20},{20... | collective-permute-start | bytes 2359304 | tf_op jit(solution)/shard_map/ppermute | solution.py:47
  61.9 48.9 %collective-permute-start.17 = (bf16[768,512]{1,0:T(8,128)(2,1)}, bf16[768,512]{1,0:T(8,128)(2,1)S(1)}, u32[]{:S(2)}, u32[]{:S(2)}) collective-permute-start(bf16[768,512]{1,0:T(8,128)(2,1)} %collective-permute-done.15), channel_id=1, source_target_pairs={{0,4},{4,8},{8,12},{12,0},{1,5},{5,9},{9,13},{13,1},{2,6},{6,10},{... | collective-permute-start | bytes 2359304 | tf_op jit(solution)/shard_map/ppermute | solution.py:45
  77.1 35.2 %collective-permute-start.10 = (bf16[512,768]{1,0:T(8,128)(2,1)S(1)}, bf16[512,768]{1,0:T(8,128)(2,1)S(1)}, u32[]{:S(2)}, u32[]{:S(2)}) collective-permute-start(bf16[512,768]{1,0:T(8,128)(2,1)S(1)} %collective-permute-done.4), channel_id=1, source_target_pairs={{0,16},{16,0},{1,17},{17,1},{2,18},{18,2},{3,19},{19,3},{4,20},{20... | collective-permute-start | bytes 2359304 | tf_op jit(solution)/shard_map/ppermute | solution.py:47
  94.0 33.7 %collective-permute-start.5 = (bf16[512,768]{1,0:T(8,128)(2,1)S(1)}, bf16[512,768]{1,0:T(8,128)(2,1)S(1)}, u32[]{:S(2)}, u32[]{:S(2)}) collective-permute-start(bf16[512,768]{1,0:T(8,128)(2,1)S(1)} %collective-permute-done.4), channel_id=1, source_target_pairs={{0,4},{4,8},{8,12},{12,0},{1,5},{5,9},{9,13},{13,1},{2,6},{6,10},{... | collective-permute-start | bytes 2359304 | tf_op jit(solution)/shard_map/ppermute | solution.py:45
  94.5 50.1 %collective-permute-start.8 = (bf16[512,768]{1,0:T(8,128)(2,1)S(1)}, bf16[512,768]{1,0:T(8,128)(2,1)S(1)}, u32[]{:S(2)}, u32[]{:S(2)}) collective-permute-start(bf16[512,768]{1,0:T(8,128)(2,1)S(1)} %collective-permute-done.7), channel_id=1, source_target_pairs={{0,4},{4,8},{8,12},{12,0},{1,5},{5,9},{9,13},{13,1},{2,6},{6,10},{... | collective-permute-start | bytes 2359304 | tf_op jit(solution)/shard_map/ppermute | solution.py:45
  110.8 51.2 %collective-permute-start.13 = (bf16[512,768]{1,0:T(8,128)(2,1)S(1)}, bf16[512,768]{1,0:T(8,128)(2,1)S(1)}, u32[]{:S(2)}, u32[]{:S(2)}) collective-permute-start(bf16[512,768]{1,0:T(8,128)(2,1)S(1)} %collective-permute-done.7), channel_id=1, source_target_pairs={{0,16},{16,0},{1,17},{17,1},{2,18},{18,2},{3,19},{19,3},{4,20},{20... | collective-permute-start | bytes 2359304 | tf_op jit(solution)/shard_map/ppermute | solution.py:47
  112.4 70.2 %collective-permute-start.18 = (bf16[768,512]{1,0:T(8,128)(2,1)S(1)}, bf16[768,512]{1,0:T(8,128)(2,1)S(1)}, u32[]{:S(2)}, u32[]{:S(2)}) collective-permute-start(bf16[768,512]{1,0:T(8,128)(2,1)S(1)} %collective-permute-done.17), channel_id=1, source_target_pairs={{0,16},{16,0},{1,17},{17,1},{2,18},{18,2},{3,19},{19,3},{4,20},{20... | collective-permute-start | bytes 2359304 | tf_op jit(solution)/shard_map/ppermute | solution.py:47
  127.7 32.4 %collective-permute-start.19 = (bf16[768,512]{1,0:T(8,128)(2,1)S(1)}, bf16[768,512]{1,0:T(8,128)(2,1)S(1)}, u32[]{:S(2)}, u32[]{:S(2)}) collective-permute-start(bf16[768,512]{1,0:T(8,128)(2,1)S(1)} %collective-permute-done.17), channel_id=1, source_target_pairs={{0,4},{4,8},{8,12},{12,0},{1,5},{5,9},{9,13},{13,1},{2,6},{6,10},{... | collective-permute-start | bytes 2359304 | tf_op jit(solution)/shard_map/ppermute | solution.py:45
  160.0 20.4 %collective-permute-start.14 = (bf16[512,768]{1,0:T(8,128)(2,1)S(1)}, bf16[512,768]{1,0:T(8,128)(2,1)S(1)}, u32[]{:S(2)}, u32[]{:S(2)}) collective-permute-start(bf16[512,768]{1,0:T(8,128)(2,1)S(1)} %collective-permute-done.8), channel_id=1, source_target_pairs={{0,16},{16,0},{1,17},{17,1},{2,18},{18,2},{3,19},{19,3},{4,20},{20... | collective-permute-start | bytes 2359304 | tf_op jit(solution)/shard_map/ppermute | solution.py:47
  162.0 33.1 %collective-permute-start.20 = (bf16[768,512]{1,0:T(8,128)(2,1)S(1)}, bf16[768,512]{1,0:T(8,128)(2,1)S(1)}, u32[]{:S(2)}, u32[]{:S(2)}) collective-permute-start(bf16[768,512]{1,0:T(8,128)(2,1)S(1)} %collective-permute-done.19), channel_id=1, source_target_pairs={{0,16},{16,0},{1,17},{17,1},{2,18},{18,2},{3,19},{19,3},{4,20},{20... | collective-permute-start | bytes 2359304 | tf_op jit(solution)/shard_map/ppermute | solution.py:47
  200.4 24.2 %collective-permute-start.33 = (bf16[256,256]{1,0:T(8,128)(2,1)}, bf16[256,256]{1,0:T(8,128)(2,1)}, u32[]{:S(2)}, u32[]{:S(2)}) collective-permute-start(bf16[256,256]{1,0:T(8,128)(2,1)} %get-tuple-element.6), channel_id=1, source_target_pairs={{0,4},{4,8},{8,12},{12,0},{1,5},{5,9},{9,13},{13,1},{2,6},{6,10},{... | collective-permute-start | bytes 393224 | tf_op jit(solution)/shard_map/ppermute | solution.py:45
  203.1 23.0 %collective-permute-start.39 = (bf16[128,512]{1,0:T(8,128)(2,1)}, bf16[128,512]{1,0:T(8,128)(2,1)}, u32[]{:S(2)}, u32[]{:S(2)}) collective-permute-start(bf16[128,512]{1,0:T(8,128)(2,1)} %get-tuple-element.21), channel_id=1, source_target_pairs={{0,4},{4,8},{8,12},{12,0},{1,5},{5,9},{9,13},{13,1},{2,6},{6,10},{... | collective-permute-start | bytes 393224 | tf_op jit(solution)/shard_map/ppermute | solution.py:45
  206.6 33.7 %collective-permute-start.27 = (bf16[256,512]{1,0:T(8,128)(2,1)}, bf16[256,512]{1,0:T(8,128)(2,1)}, u32[]{:S(2)}, u32[]{:S(2)}) collective-permute-start(bf16[256,512]{1,0:T(8,128)(2,1)} %get-tuple-element.10), channel_id=1, source_target_pairs={{0,4},{4,8},{8,12},{12,0},{1,5},{5,9},{9,13},{13,1},{2,6},{6,10},{... | collective-permute-start | bytes 786440 | tf_op jit(solution)/shard_map/ppermute | solution.py:45
  208.2 20.0 %collective-permute-start.23 = (bf16[384,512]{1,0:T(8,128)(2,1)}, bf16[384,512]{1,0:T(8,128)(2,1)}, u32[]{:S(2)}, u32[]{:S(2)}) collective-permute-start(bf16[384,512]{1,0:T(8,128)(2,1)} %get-tuple-element.18), channel_id=1, source_target_pairs={{0,1},{1,0},{2,3},{3,2},{4,5},{5,4},{6,7},{7,6},{8,9},{9,8},{10,11... | collective-permute-start | bytes 1179656 | tf_op jit(solution)/shard_map/ppermute | solution.py:84
  230.5 19.7 %collective-permute-start.25 = (bf16[384,512]{1,0:T(8,128)(2,1)S(1)}, bf16[384,512]{1,0:T(8,128)(2,1)S(1)}, u32[]{:S(2)}, u32[]{:S(2)}) collective-permute-start(bf16[384,512]{1,0:T(8,128)(2,1)S(1)} %get-tuple-element.8), channel_id=1, source_target_pairs={{0,2},{1,3},{2,0},{3,1},{4,6},{5,7},{6,4},{7,5},{8,10},{9,11},{10,... | collective-permute-start | bytes 1179656 | tf_op jit(solution)/shard_map/ppermute | solution.py:67
  240.4 22.4 %collective-permute-start.24 = (bf16[384,512]{1,0:T(8,128)(2,1)S(1)}, bf16[384,512]{1,0:T(8,128)(2,1)S(1)}, u32[]{:S(2)}, u32[]{:S(2)}) collective-permute-start(bf16[384,512]{1,0:T(8,128)(2,1)S(1)} %get-tuple-element.8), channel_id=1, source_target_pairs={{0,1},{1,0},{2,3},{3,2},{4,5},{5,4},{6,7},{7,6},{8,9},{9,8},{10,11... | collective-permute-start | bytes 1179656 | tf_op jit(solution)/shard_map/ppermute | solution.py:65
  252.8 21.9 %collective-permute-start.29 = (bf16[256,512]{1,0:T(8,128)(2,1)}, bf16[256,512]{1,0:T(8,128)(2,1)}, u32[]{:S(2)}, u32[]{:S(2)}) collective-permute-start(bf16[256,512]{1,0:T(8,128)(2,1)} %collective-permute-done.27), channel_id=1, source_target_pairs={{0,4},{4,8},{8,12},{12,0},{1,5},{5,9},{9,13},{13,1},{2,6},{6,10},{... | collective-permute-start | bytes 786440 | tf_op jit(solution)/shard_map/ppermute | solution.py:45
  (80 other events, 661.7 us)
where the time goes:
time: 358 us; the launch traced here: 357 us
  waiting for transfers between devices  181 us (51%)
  local copies, waits for them, and re-layouts  57.1 us (16%)
  starting transfers between devices  46.8 us (13%)
  matrix products  42.7 us (12%)
  blocking collectives  21.1 us (6%)
  other arithmetic  6.21 us (2%)
    ppermute x18, waiting for transfers between devices, pieces_of(): current = lax.ppermute(current, 'fs', shift(n_fs, 1))  114 us
    ppermute x18, waiting for transfers between devices, pieces_of(): lax.ppermute(current, 'grp', shift(n_grp, k))  38.5 us
    dynamic_update_slice x23, local copies, waits for them, and re-layouts, absolute(): whole = lax.dynamic_update_slice(whole, part, start)  33.3 us
    ppermute x18, starting transfers between devices, pieces_of(): lax.ppermute(current, 'grp', shift(n_grp, k))  22.2 us
    all_gather x3, blocking collectives, norm_rows(): gain_whole = lax.all_gather(gain, 'tp', axis=1, tiled=True)  21.1 us
    dot_general x32, matrix products, project(): jnp.dot(inputs[s], gathered[s][k], preferred_element_type=jnp.float32)  20.7 us
    ppermute x18, starting transfers between devices, pieces_of(): current = lax.ppermute(current, 'fs', shift(n_fs, 1))  15.6 us
    ppermute x3, waiting for transfers between devices, gather_tp(): far = lax.ppermute(value, 'tp', shift(n_tp, 2 * k))  14.2 us
  transfers between devices with their start and end apart: 54, of which 20 were waited for; matrix products, arithmetic and copies ran while one was open for 20% of the time, Pallas kernels for 0%

commit v1 on v0

--- a/solution.py
+++ b/solution.py
@@ -1,7 +1,37 @@
+import functools
 import jax
 import jax.numpy as jnp
 from jax import lax
 from jax.sharding import PartitionSpec as P
+from jax.lax import axis_index, axis_size, ppermute
+
+
+def post_the_packet(buf, mesh_dim):
+    ready, known, kept_arr = (axis_size(mesh_dim), axis_index(mesh_dim), buf.shape[1])
+    so_far_all = []
+    for ii in [*range(ready)]:
+        so_far_all.append((ii, (ii + 1) % ready))
+    panels = []
+    for ii in tuple(range(ready)):
+        panels.append((ii, (ii - 1) % ready))
+    spare = jnp.zeros((*buf.shape[:1], ready * kept_arr, *buf.shape[2:]), buf.dtype)
+    spare = lax.dynamic_update_slice_in_dim(spare, buf, known * kept_arr, axis=1)
+    piece_now = u_next = buf
+    u1 = ready // 2
+    for dev_i in [*range(1, u1 + 1)]:
+        piece_now = ppermute(piece_now, mesh_dim, so_far_all)
+        spare = lax.dynamic_update_slice_in_dim(
+            spare, piece_now, (known - dev_i) % ready * kept_arr, axis=1
+        )
+        if dev_i < ready - u1:
+            u_next = ppermute(u_next, mesh_dim, panels)
+            spare = lax.dynamic_update_slice_in_dim(
+                spare, u_next, (known + dev_i) % ready * kept_arr, axis=1
+            )
+    return spare
+
+
+change_circles_for = functools.partial(post_the_packet, mesh_dim="tp")
 
 
 def shift(size, step):
@@ -92,7 +122,7 @@
 
     def norm_rows(values, gain):
         whole = gather_tp(values)
-        gain_whole = lax.all_gather(gain, "tp", axis=1, tiled=True)
+        gain_whole = change_circles_for(gain)
         widened = whole.astype(jnp.float32)
         scaled = (widened * gain_whole.astype(jnp.float32)).astype(jnp.bfloat16)
         factor = lax.rsqrt(jnp.mean(widened * widened, axis=1, keepdims=True) + 1e-06)

time: 358 us -> 369 us (1.031)
  blocking collectives: 21.1 us -> 0 us
  local copies, waits for them, and re-layouts: 57.1 us -> 71.9 us
  other arithmetic: 6.21 us -> 14 us
  starting transfers between devices: 46.8 us -> 54 us
    all_gather x3 -> x0, blocking collectives: 21.1 us -> none  [norm_rows(): gain_whole = lax.all_gather(gain, 'tp', axis=1, tiled=True)]
    dynamic_update_slice x10, local copies, waits for them, and re-layouts: 3.43 us -> 11.8 us  [gather_tp(): whole = lax.dynamic_update_slice(whole, piece, (0, source * value.shape[1]))]
    ppermute x0 -> x9, waiting for transfers between devices: none -> 7.61 us  [the longest x3 4.12 us: post_the_packet(): u_next = ppermute(u_next, mesh_dim, panels)]
    ppermute x0 -> x9, starting transfers between devices: none -> 6.4 us  [the longest x6 3.59 us: post_the_packet(): piece_now = ppermute(piece_now, mesh_dim, so_far_all)]
    ppermute x18, waiting for transfers between devices: 114 us -> 109 us  [pieces_of(): current = lax.ppermute(current, 'fs', shift(n_fs, 1))]
    ppermute x0 -> x9, other arithmetic: none -> 4.23 us  [the longest x6 2.16 us: post_the_packet(): piece_now = ppermute(piece_now, mesh_dim, so_far_all)]
    unnamed x100 -> x106, local copies, waits for them, and re-layouts: 10.8 us -> 13 us
  transfers between devices with their start and end apart: 54 -> 63, of which waited for: 20 -> 25; matrix products, arithmetic and copies ran while one was open for 20% -> 25% of each run, Pallas kernels for 0% -> 0%
where the time goes in v1:
time: 369 us; the launch traced here: 368 us
  waiting for transfers between devices  184 us (50%)
  local copies, waits for them, and re-layouts  71.9 us (19%)
  starting transfers between devices  54 us (15%)
  matrix products  42 us (11%)
  other arithmetic  14 us (4%)
    ppermute x18, waiting for transfers between devices, pieces_of(): current = lax.ppermute(current, 'fs', shift(n_fs, 1))  109 us
    ppermute x18, waiting for transfers between devices, pieces_of(): lax.ppermute(current, 'grp', shift(n_grp, k))  40.1 us
    dynamic_update_slice x23, local copies, waits for them, and re-layouts, absolute(): whole = lax.dynamic_update_slice(whole, part, start)  32.5 us
    ppermute x18, starting transfers between devices, pieces_of(): lax.ppermute(current, 'grp', shift(n_grp, k))  21.6 us
    dot_general x32, matrix products, project(): jnp.dot(inputs[s], gathered[s][k], preferred_element_type=jnp.float32)  20.8 us
    ppermute x18, starting transfers between devices, pieces_of(): current = lax.ppermute(current, 'fs', shift(n_fs, 1))  16.3 us
    ppermute x3, waiting for transfers between devices, gather_tp(): far = lax.ppermute(value, 'tp', shift(n_tp, 2 * k))  13.3 us
    ppermute x3, waiting for transfers between devices, scatter_tp(): lax.ppermute(pair.astype(jnp.bfloat16), 'tp', shift(n_tp, 2 * k))  13.1 us
  transfers between devices with their start and end apart: 63, of which 25 were waited for; matrix products, arithmetic and copies ran while one was open for 25% of the time, Pallas kernels for 0%

profile of v1, /device:TPU:0, one launch (start us, length us, event | category | flops | bytes accessed | tf_op | source)
XLA Modules:
  0.0 367.5 jit_solution(2295992860970621199)
XLA Ops:
  0.0 3.0 collective-permute-start.1
  8.9 3.6 collective-permute-done.1
  33.5 9.9 %collective-permute-done.9 = bf16[512,768]{1,0:T(8,128)(2,1)} collective-permute-done((bf16[512,768]{1,0:T(8,128)(2,1)S(1)}, bf16[512,768]{1,0:T(8,128)(2,1)}, u32[]{:S(2)}, u32[]{:S(2)}) %collective-permute-start.9) | collective-permute-done | bytes 786464 | tf_op jit(solution)/shard_map/ppermute | solution.py:75
  49.4 10.9 %collective-permute-done.18 = bf16[768,512]{1,0:T(8,128)(2,1)} collective-permute-done((bf16[768,512]{1,0:T(8,128)(2,1)}, bf16[768,512]{1,0:T(8,128)(2,1)}, u32[]{:S(2)}, u32[]{:S(2)}) %collective-permute-start.18) | collective-permute-done | bytes 786464 | tf_op jit(solution)/shard_map/ppermute | solution.py:75
  61.9 15.1 %collective-permute-done.7 = bf16[512,768]{1,0:T(8,128)(2,1)S(1)} collective-permute-done((bf16[512,768]{1,0:T(8,128)(2,1)}, bf16[512,768]{1,0:T(8,128)(2,1)S(1)}, u32[]{:S(2)}, u32[]{:S(2)}) %collective-permute-start.7) | collective-permute-done | bytes 786464 | tf_op jit(solution)/shard_map/ppermute | solution.py:75
  79.5 14.4 %collective-permute-done.10 = bf16[512,768]{1,0:T(8,128)(2,1)S(1)} collective-permute-done((bf16[512,768]{1,0:T(8,128)(2,1)}, bf16[512,768]{1,0:T(8,128)(2,1)S(1)}, u32[]{:S(2)}, u32[]{:S(2)}) %collective-permute-start.10) | collective-permute-done | bytes 786464 | tf_op jit(solution)/shard_map/ppermute | solution.py:75
  96.3 14.5 %collective-permute-done.20 = bf16[768,512]{1,0:T(8,128)(2,1)S(1)} collective-permute-done((bf16[768,512]{1,0:T(8,128)(2,1)}, bf16[768,512]{1,0:T(8,128)(2,1)S(1)}, u32[]{:S(2)}, u32[]{:S(2)}) %collective-permute-start.20) | collective-permute-done | bytes 786464 | tf_op jit(solution)/shard_map/ppermute | solution.py:75
  113.4 14.2 %collective-permute-done.8 = bf16[512,768]{1,0:T(8,128)(2,1)S(1)} collective-permute-done((bf16[512,768]{1,0:T(8,128)(2,1)S(1)}, bf16[512,768]{1,0:T(8,128)(2,1)S(1)}, u32[]{:S(2)}, u32[]{:S(2)}) %collective-permute-start.8) | collective-permute-done | bytes 786464 | tf_op jit(solution)/shard_map/ppermute | solution.py:75
  128.2 16.3 %collective-permute-done.11 = bf16[512,768]{1,0:T(8,128)(2,1)S(1)} collective-permute-done((bf16[512,768]{1,0:T(8,128)(2,1)S(1)}, bf16[512,768]{1,0:T(8,128)(2,1)S(1)}, u32[]{:S(2)}, u32[]{:S(2)}) %collective-permute-start.11) | collective-permute-done | bytes 786464 | tf_op jit(solution)/shard_map/ppermute | solution.py:75
  149.2 10.8 %collective-permute-done.22 = bf16[768,512]{1,0:T(8,128)(2,1)S(1)} collective-permute-done((bf16[768,512]{1,0:T(8,128)(2,1)S(1)}, bf16[768,512]{1,0:T(8,128)(2,1)S(1)}, u32[]{:S(2)}, u32[]{:S(2)}) %collective-permute-start.22) | collective-permute-done | bytes 786464 | tf_op jit(solution)/shard_map/ppermute | solution.py:75
  164.0 16.4 %collective-permute-done.17 = bf16[512,768]{1,0:T(8,128)(2,1)S(1)} collective-permute-done((bf16[512,768]{1,0:T(8,128)(2,1)S(1)}, bf16[512,768]{1,0:T(8,128)(2,1)S(1)}, u32[]{:S(2)}, u32[]{:S(2)}) %collective-permute-start.17) | collective-permute-done | bytes 786464 | tf_op jit(solution)/shard_map/ppermute | solution.py:77
  183.0 12.1 %collective-permute-done.23 = bf16[768,512]{1,0:T(8,128)(2,1)S(1)} collective-permute-done((bf16[768,512]{1,0:T(8,128)(2,1)S(1)}, bf16[768,512]{1,0:T(8,128)(2,1)S(1)}, u32[]{:S(2)}, u32[]{:S(2)}) %collective-permute-start.23) | collective-permute-done | bytes 786464 | tf_op jit(solution)/shard_map/ppermute | solution.py:77
  214.5 4.1 %collective-permute-done.31 = bf16[1,512]{1,0:T(2,128)(2,1)S(1)} collective-permute-done((bf16[1,512]{1,0:T(2,128)(2,1)S(1)}, bf16[1,512]{1,0:T(2,128)(2,1)S(1)}, u32[]{:S(2)}, u32[]{:S(2)}) %collective-permute-start.31) | collective-permute-done | bytes 1056 | tf_op jit(solution)/shard_map/ppermute | solution.py:27
  233.5 2.9 dynamic_update_slice.218
  243.8 3.5 dynamic_update_slice.220
  257.0 3.4 dynamic_update_slice.222
  264.6 2.5 fusion.61
  273.3 3.3 collective-permute-start.34
  279.2 4.9 %collective-permute-done.34 = bf16[256,512]{1,0:T(8,128)(2,1)S(1)} collective-permute-done((bf16[256,512]{1,0:T(8,128)(2,1)}, bf16[256,512]{1,0:T(8,128)(2,1)S(1)}, u32[]{:S(2)}, u32[]{:S(2)}) %collective-permute-start.34) | collective-permute-done | bytes 262176 | tf_op jit(solution)/shard_map/ppermute | solution.py:77
  291.1 3.9 %collective-permute-done.38 = bf16[256,512]{1,0:T(8,128)(2,1)S(1)} collective-permute-done((bf16[256,512]{1,0:T(8,128)(2,1)S(1)}, bf16[256,512]{1,0:T(8,128)(2,1)S(1)}, u32[]{:S(2)}, u32[]{:S(2)}) %collective-permute-start.38) | collective-permute-done | bytes 262176 | tf_op jit(solution)/shard_map/ppermute | solution.py:77
  295.8 3.1 collective-permute-done.52
  299.1 2.8 constant_dynamic-update-slice_fusion.3
  304.2 9.7 %collective-permute-done.55 = bf16[384,512]{1,0:T(8,128)(2,1)} collective-permute-done((bf16[384,512]{1,0:T(8,128)(2,1)S(1)}, bf16[384,512]{1,0:T(8,128)(2,1)}, u32[]{:S(2)}, u32[]{:S(2)}) %collective-permute-start.55) | collective-permute-done | bytes 393248 | tf_op jit(solution)/shard_map/ppermute | solution.py:97
  356.5 10.0 %collective-permute-done.61 = bf16[384,512]{1,0:T(8,128)(2,1)S(1)} collective-permute-done((bf16[384,512]{1,0:T(8,128)(2,1)S(1)}, bf16[384,512]{1,0:T(8,128)(2,1)S(1)}, u32[]{:S(2)}, u32[]{:S(2)}) %collective-permute-start.61) | collective-permute-done | bytes 393248 | tf_op jit(solution)/shard_map/ppermute | solution.py:117
  (352 shorter events, 171.1 us)
Async XLA Ops:
  4.2 22.4 %collective-permute-start.6 = (bf16[512,768]{1,0:T(8,128)(2,1)S(1)}, bf16[512,768]{1,0:T(8,128)(2,1)}, u32[]{:S(2)}, u32[]{:S(2)}) collective-permute-start(bf16[512,768]{1,0:T(8,128)(2,1)S(1)} %constant_dynamic-slice_fusion.11), channel_id=1, source_target_pairs={{0,4},{4,8},{8,12},{12,0},{1,5},{5,9},{9,13},{13,1},{2,6},{6,10},{... | collective-permute-start | bytes 2359304 | tf_op jit(solution)/shard_map/ppermute | solution.py:75
  16.7 26.7 %collective-permute-start.9 = (bf16[512,768]{1,0:T(8,128)(2,1)S(1)}, bf16[512,768]{1,0:T(8,128)(2,1)}, u32[]{:S(2)}, u32[]{:S(2)}) collective-permute-start(bf16[512,768]{1,0:T(8,128)(2,1)S(1)} %constant_dynamic-slice_fusion.10), channel_id=1, source_target_pairs={{0,4},{4,8},{8,12},{12,0},{1,5},{5,9},{9,13},{13,1},{2,6},{6,10},{... | collective-permute-start | bytes 2359304 | tf_op jit(solution)/shard_map/ppermute | solution.py:75
  19.5 40.8 %collective-permute-start.18 = (bf16[768,512]{1,0:T(8,128)(2,1)}, bf16[768,512]{1,0:T(8,128)(2,1)}, u32[]{:S(2)}, u32[]{:S(2)}) collective-permute-start(bf16[768,512]{1,0:T(8,128)(2,1)} %constant_dynamic-slice_fusion.9), channel_id=1, source_target_pairs={{0,4},{4,8},{8,12},{12,0},{1,5},{5,9},{9,13},{13,1},{2,6},{6,10},{... | collective-permute-start | bytes 2359304 | tf_op jit(solution)/shard_map/ppermute | solution.py:75
  26.6 35.2 %collective-permute-start.12 = (bf16[512,768]{1,0:T(8,128)(2,1)}, bf16[512,768]{1,0:T(8,128)(2,1)S(1)}, u32[]{:S(2)}, u32[]{:S(2)}) collective-permute-start(bf16[512,768]{1,0:T(8,128)(2,1)} %collective-permute-done.6), channel_id=1, source_target_pairs={{0,16},{16,0},{1,17},{17,1},{2,18},{18,2},{3,19},{19,3},{4,20},{20... | collective-permute-start | bytes 2359304 | tf_op jit(solution)/shard_map/ppermute | solution.py:77
  28.1 48.9 %collective-permute-start.7 = (bf16[512,768]{1,0:T(8,128)(2,1)}, bf16[512,768]{1,0:T(8,128)(2,1)S(1)}, u32[]{:S(2)}, u32[]{:S(2)}) collective-permute-start(bf16[512,768]{1,0:T(8,128)(2,1)} %collective-permute-done.6), channel_id=1, source_target_pairs={{0,4},{4,8},{8,12},{12,0},{1,5},{5,9},{9,13},{13,1},{2,6},{6,10},{... | collective-permute-start | bytes 2359304 | tf_op jit(solution)/shard_map/ppermute | solution.py:75
  43.5 50.5 %collective-permute-start.10 = (bf16[512,768]{1,0:T(8,128)(2,1)}, bf16[512,768]{1,0:T(8,128)(2,1)S(1)}, u32[]{:S(2)}, u32[]{:S(2)}) collective-permute-start(bf16[512,768]{1,0:T(8,128)(2,1)} %collective-permute-done.9), channel_id=1, source_target_pairs={{0,4},{4,8},{8,12},{12,0},{1,5},{5,9},{9,13},{13,1},{2,6},{6,10},{... | collective-permute-start | bytes 2359304 | tf_op jit(solution)/shard_map/ppermute | solution.py:75
  47.8 46.6 %collective-permute-start.15 = (bf16[512,768]{1,0:T(8,128)(2,1)}, bf16[512,768]{1,0:T(8,128)(2,1)S(1)}, u32[]{:S(2)}, u32[]{:S(2)}) collective-permute-start(bf16[512,768]{1,0:T(8,128)(2,1)} %collective-permute-done.9), channel_id=1, source_target_pairs={{0,16},{16,0},{1,17},{17,1},{2,18},{18,2},{3,19},{19,3},{4,20},{20... | collective-permute-start | bytes 2359304 | tf_op jit(solution)/shard_map/ppermute | solution.py:77
  60.3 121.7 %collective-permute-start.19 = (bf16[768,512]{1,0:T(8,128)(2,1)}, bf16[768,512]{1,0:T(8,128)(2,1)S(1)}, u32[]{:S(2)}, u32[]{:S(2)}) collective-permute-start(bf16[768,512]{1,0:T(8,128)(2,1)} %collective-permute-done.18), channel_id=1, source_target_pairs={{0,16},{16,0},{1,17},{17,1},{2,18},{18,2},{3,19},{19,3},{4,20},{20... | collective-permute-start | bytes 2359304 | tf_op jit(solution)/shard_map/ppermute | solution.py:77
  61.8 48.9 %collective-permute-start.20 = (bf16[768,512]{1,0:T(8,128)(2,1)}, bf16[768,512]{1,0:T(8,128)(2,1)S(1)}, u32[]{:S(2)}, u32[]{:S(2)}) collective-permute-start(bf16[768,512]{1,0:T(8,128)(2,1)} %collective-permute-done.18), channel_id=1, source_target_pairs={{0,4},{4,8},{8,12},{12,0},{1,5},{5,9},{9,13},{13,1},{2,6},{6,10},{... | collective-permute-start | bytes 2359304 | tf_op jit(solution)/shard_map/ppermute | solution.py:75
  77.1 35.2 %collective-permute-start.13 = (bf16[512,768]{1,0:T(8,128)(2,1)S(1)}, bf16[512,768]{1,0:T(8,128)(2,1)S(1)}, u32[]{:S(2)}, u32[]{:S(2)}) collective-permute-start(bf16[512,768]{1,0:T(8,128)(2,1)S(1)} %collective-permute-done.7), channel_id=1, source_target_pairs={{0,16},{16,0},{1,17},{17,1},{2,18},{18,2},{3,19},{19,3},{4,20},{20... | collective-permute-start | bytes 2359304 | tf_op jit(solution)/shard_map/ppermute | solution.py:77
  93.9 33.7 %collective-permute-start.8 = (bf16[512,768]{1,0:T(8,128)(2,1)S(1)}, bf16[512,768]{1,0:T(8,128)(2,1)S(1)}, u32[]{:S(2)}, u32[]{:S(2)}) collective-permute-start(bf16[512,768]{1,0:T(8,128)(2,1)S(1)} %collective-permute-done.7), channel_id=1, source_target_pairs={{0,4},{4,8},{8,12},{12,0},{1,5},{5,9},{9,13},{13,1},{2,6},{6,10},{... | collective-permute-start | bytes 2359304 | tf_op jit(solution)/shard_map/ppermute | solution.py:75
  94.4 50.1 %collective-permute-start.11 = (bf16[512,768]{1,0:T(8,128)(2,1)S(1)}, bf16[512,768]{1,0:T(8,128)(2,1)S(1)}, u32[]{:S(2)}, u32[]{:S(2)}) collective-permute-start(bf16[512,768]{1,0:T(8,128)(2,1)S(1)} %collective-permute-done.10), channel_id=1, source_target_pairs={{0,4},{4,8},{8,12},{12,0},{1,5},{5,9},{9,13},{13,1},{2,6},{6,10},{... | collective-permute-start | bytes 2359304 | tf_op jit(solution)/shard_map/ppermute | solution.py:75
  110.8 51.2 %collective-permute-start.16 = (bf16[512,768]{1,0:T(8,128)(2,1)S(1)}, bf16[512,768]{1,0:T(8,128)(2,1)S(1)}, u32[]{:S(2)}, u32[]{:S(2)}) collective-permute-start(bf16[512,768]{1,0:T(8,128)(2,1)S(1)} %collective-permute-done.10), channel_id=1, source_target_pairs={{0,16},{16,0},{1,17},{17,1},{2,18},{18,2},{3,19},{19,3},{4,20},{20... | collective-permute-start | bytes 2359304 | tf_op jit(solution)/shard_map/ppermute | solution.py:77
  112.3 70.2 %collective-permute-start.21 = (bf16[768,512]{1,0:T(8,128)(2,1)S(1)}, bf16[768,512]{1,0:T(8,128)(2,1)S(1)}, u32[]{:S(2)}, u32[]{:S(2)}) collective-permute-start(bf16[768,512]{1,0:T(8,128)(2,1)S(1)} %collective-permute-done.20), channel_id=1, source_target_pairs={{0,16},{16,0},{1,17},{17,1},{2,18},{18,2},{3,19},{19,3},{4,20},{20... | collective-permute-start | bytes 2359304 | tf_op jit(solution)/shard_map/ppermute | solution.py:77
  127.6 32.4 %collective-permute-start.22 = (bf16[768,512]{1,0:T(8,128)(2,1)S(1)}, bf16[768,512]{1,0:T(8,128)(2,1)S(1)}, u32[]{:S(2)}, u32[]{:S(2)}) collective-permute-start(bf16[768,512]{1,0:T(8,128)(2,1)S(1)} %collective-permute-done.20), channel_id=1, source_target_pairs={{0,4},{4,8},{8,12},{12,0},{1,5},{5,9},{9,13},{13,1},{2,6},{6,10},{... | collective-permute-start | bytes 2359304 | tf_op jit(solution)/shard_map/ppermute | solution.py:75
  160.0 20.4 %collective-permute-start.17 = (bf16[512,768]{1,0:T(8,128)(2,1)S(1)}, bf16[512,768]{1,0:T(8,128)(2,1)S(1)}, u32[]{:S(2)}, u32[]{:S(2)}) collective-permute-start(bf16[512,768]{1,0:T(8,128)(2,1)S(1)} %collective-permute-done.11), channel_id=1, source_target_pairs={{0,16},{16,0},{1,17},{17,1},{2,18},{18,2},{3,19},{19,3},{4,20},{20... | collective-permute-start | bytes 2359304 | tf_op jit(solution)/shard_map/ppermute | solution.py:77
  162.0 33.1 %collective-permute-start.23 = (bf16[768,512]{1,0:T(8,128)(2,1)S(1)}, bf16[768,512]{1,0:T(8,128)(2,1)S(1)}, u32[]{:S(2)}, u32[]{:S(2)}) collective-permute-start(bf16[768,512]{1,0:T(8,128)(2,1)S(1)} %collective-permute-done.22), channel_id=1, source_target_pairs={{0,16},{16,0},{1,17},{17,1},{2,18},{18,2},{3,19},{19,3},{4,20},{20... | collective-permute-start | bytes 2359304 | tf_op jit(solution)/shard_map/ppermute | solution.py:77
  200.3 24.4 %collective-permute-start.39 = (bf16[256,256]{1,0:T(8,128)(2,1)}, bf16[256,256]{1,0:T(8,128)(2,1)}, u32[]{:S(2)}, u32[]{:S(2)}) collective-permute-start(bf16[256,256]{1,0:T(8,128)(2,1)} %get-tuple-element.6), channel_id=1, source_target_pairs={{0,4},{4,8},{8,12},{12,0},{1,5},{5,9},{9,13},{13,1},{2,6},{6,10},{... | collective-permute-start | bytes 393224 | tf_op jit(solution)/shard_map/ppermute | solution.py:75
  203.6 22.6 %collective-permute-start.45 = (bf16[128,512]{1,0:T(8,128)(2,1)}, bf16[128,512]{1,0:T(8,128)(2,1)}, u32[]{:S(2)}, u32[]{:S(2)}) collective-permute-start(bf16[128,512]{1,0:T(8,128)(2,1)} %get-tuple-element.21), channel_id=1, source_target_pairs={{0,4},{4,8},{8,12},{12,0},{1,5},{5,9},{9,13},{13,1},{2,6},{6,10},{... | collective-permute-start | bytes 393224 | tf_op jit(solution)/shard_map/ppermute | solution.py:75
  206.1 22.3 %collective-permute-start.26 = (bf16[384,512]{1,0:T(8,128)(2,1)}, bf16[384,512]{1,0:T(8,128)(2,1)}, u32[]{:S(2)}, u32[]{:S(2)}) collective-permute-start(bf16[384,512]{1,0:T(8,128)(2,1)} %get-tuple-element.18), channel_id=1, source_target_pairs={{0,1},{1,0},{2,3},{3,2},{4,5},{5,4},{6,7},{7,6},{8,9},{9,8},{10,11... | collective-permute-start | bytes 1179656 | tf_op jit(solution)/shard_map/ppermute | solution.py:114
  208.2 20.7 %collective-permute-start.25 = (bf16[384,512]{1,0:T(8,128)(2,1)}, bf16[384,512]{1,0:T(8,128)(2,1)}, u32[]{:S(2)}, u32[]{:S(2)}) collective-permute-start(bf16[384,512]{1,0:T(8,128)(2,1)} %add_convert_fusion.4), channel_id=1, source_target_pairs={{0,2},{1,3},{2,0},{3,1},{4,6},{5,7},{6,4},{7,5},{8,10},{9,11},{10,... | collective-permute-start | bytes 1179656 | tf_op jit(solution)/shard_map/ppermute | solution.py:117
  231.0 19.7 %collective-permute-start.28 = (bf16[384,512]{1,0:T(8,128)(2,1)S(1)}, bf16[384,512]{1,0:T(8,128)(2,1)S(1)}, u32[]{:S(2)}, u32[]{:S(2)}) collective-permute-start(bf16[384,512]{1,0:T(8,128)(2,1)S(1)} %get-tuple-element.8), channel_id=1, source_target_pairs={{0,2},{1,3},{2,0},{3,1},{4,6},{5,7},{6,4},{7,5},{8,10},{9,11},{10,... | collective-permute-start | bytes 1179656 | tf_op jit(solution)/shard_map/ppermute | solution.py:97
  241.1 22.1 %collective-permute-start.27 = (bf16[384,512]{1,0:T(8,128)(2,1)S(1)}, bf16[384,512]{1,0:T(8,128)(2,1)S(1)}, u32[]{:S(2)}, u32[]{:S(2)}) collective-permute-start(bf16[384,512]{1,0:T(8,128)(2,1)S(1)} %get-tuple-element.8), channel_id=1, source_target_pairs={{0,1},{1,0},{2,3},{3,2},{4,5},{5,4},{6,7},{7,6},{8,9},{9,8},{10,11... | collective-permute-start | bytes 1179656 | tf_op jit(solution)/shard_map/ppermute | solution.py:95
  253.7 23.0 %collective-permute-start.35 = (bf16[256,512]{1,0:T(8,128)(2,1)}, bf16[256,512]{1,0:T(8,128)(2,1)S(1)}, u32[]{:S(2)}, u32[]{:S(2)}) collective-permute-start(bf16[256,512]{1,0:T(8,128)(2,1)} %collective-permute-done.33), channel_id=1, source_target_pairs={{0,4},{4,8},{8,12},{12,0},{1,5},{5,9},{9,13},{13,1},{2,6},{6,10},{... | collective-permute-start | bytes 786440 | tf_op jit(solution)/shard_map/ppermute | solution.py:75
  (92 other events, 724.4 us)
